TPU v7x, 32 devices: a whole 2x2x4 slice. The times are simulated.
32 devices in a mesh: fs: 8 (over z, y), tp: 4 (over x, core).
Axes of the slice: x: 2, y: 2, z: 4, core: 2. Of those that a mesh axis runs over, the one named last changes fastest.
Arguments:
- tokens: bfloat16 [8192, 2048], P('fs', 'tp'), may hold values from -6 to 6
- mixer_gain: float32 [2048], replicated, may hold values from 0.1 to 1.9
- ffn_gain: float32 [2048], replicated, may hold values from 0.1 to 1.9
- w_outer: float32 [2048, 1024], P('fs', 'tp'), may hold values from -0.125 to 0.125
- w_inner: float32 [2048, 1024], P('fs', 'tp'), may hold values from -0.125 to 0.125
- w_value: float32 [2048, 1024], P('fs', 'tp'), may hold values from -0.125 to 0.125
- scale_outer: float32 [1, 1024], P(None, 'tp'), may hold values from 0.5 to 2
- scale_inner: float32 [1, 1024], P(None, 'tp'), may hold values from 0.5 to 2
- scale_value: float32 [1, 1024], P(None, 'tp'), may hold values from 0.5 to 2
- conv_taps: float32 [3, 1024], P(None, 'tp'), may hold values from -3.5 to 3.5
- w_mixout: float32 [1024, 2048], P('tp', 'fs'), may hold values from -0.1875 to 0.1875
- scale_mixout: float32 [1, 2048], P(None, 'fs'), may hold values from 0.5 to 2
- w_gate: float32 [2048, 5632], P('fs', 'tp'), may hold values from -0.125 to 0.125
- w_upward: float32 [2048, 5632], P('fs', 'tp'), may hold values from -0.125 to 0.125
- scale_gate: float32 [1, 5632], P(None, 'tp'), may hold values from 0.5 to 2
- scale_upward: float32 [1, 5632], P(None, 'tp'), may hold values from 0.5 to 2
- w_down: float32 [5632, 2048], P('tp', 'fs'), may hold values from -0.078125 to 0.078125
- scale_down: float32 [1, 2048], P(None, 'fs'), may hold values from 0.5 to 2
Outputs:
- block_out: bfloat16 [8192, 2048], P('fs', 'tp')
All inputs are finite; a program needn't handle non-finite values.
Results may differ from a plain program's by a relative error of at most 0.019.
Values may be sent and summed in bfloat16 or wider, within the bound.
No kernel may reach another device: no remote copies, remote signals or barrier semaphores. Data moves between devices by JAX's collectives and lax.ppermute only.
A program may use at most 128 MiB of HBM per device.

v0:
```python
import jax
import jax.numpy as jnp
from jax import lax
from jax.sharding import PartitionSpec as P

SEQ_LEN = 128


def rms_scaled(full_rows, gain_vec):
    values = full_rows.astype(jnp.float32)
    inverse = lax.rsqrt(jnp.mean(values * values, axis=-1, keepdims=True) + 1e-06)
    return (values * inverse * gain_vec).astype(jnp.bfloat16)


def add_rows(left, w_piece):
    return jnp.dot(left, w_piece, preferred_element_type=jnp.float32)


def causal_taps(product, conv_taps):
    padded = jnp.pad(product, ((0, 0), (conv_taps.shape[0] - 1, 0), (0, 0)))
    length = product.shape[1]
    summed = jnp.zeros(product.shape, jnp.float32)
    for tap_index in range(conv_taps.shape[0]):
        summed = summed + conv_taps[tap_index] * padded[:, tap_index : tap_index + length, :]
    return summed


def per_device(
    tokens,
    mixer_gain,
    ffn_gain,
    w_outer,
    w_inner,
    w_value,
    scale_outer,
    scale_inner,
    scale_value,
    conv_taps,
    w_mixout,
    scale_mixout,
    w_gate,
    w_upward,
    scale_gate,
    scale_upward,
    w_down,
    scale_down,
):
    full_rows = lax.all_gather(tokens, "tp", axis=1, tiled=True)
    normed = rms_scaled(full_rows, mixer_gain)
    tok_count = tokens.shape[0]
    local_channels = w_outer.shape[1]

    def add_one(w_piece):
        return add_rows(normed, w_piece)

    outer_bf = w_outer.astype(jnp.bfloat16)
    inner_bf = w_inner.astype(jnp.bfloat16)
    value_bf = w_value.astype(jnp.bfloat16)
    outer = add_one(lax.all_gather(outer_bf, "fs", axis=0, tiled=True))
    inner = add_one(lax.all_gather(inner_bf, "fs", axis=0, tiled=True))
    value = add_one(lax.all_gather(value_bf, "fs", axis=0, tiled=True))
    outer = outer * scale_outer
    product = inner * scale_inner * (value * scale_value)
    product = product.reshape(tok_count // SEQ_LEN, SEQ_LEN, local_channels)
    conv = causal_taps(product, conv_taps).reshape(tok_count, local_channels)
    mixed_out = (outer * conv).astype(jnp.bfloat16)
    mixout_scales, down_scales = (
        lax.all_gather(scale_mixout, "fs", axis=1, tiled=True),
        lax.all_gather(scale_down, "fs", axis=1, tiled=True),
    )
    mixout_bf = w_mixout.astype(jnp.bfloat16)
    mixed_all = lax.all_gather(mixed_out, "tp", axis=1, tiled=True)
    mixout_cols = lax.all_gather(mixout_bf, "fs", axis=1, tiled=True)
    mixout_all = lax.all_gather(mixout_cols, "tp", axis=0, tiled=True)
    mix_term = jnp.dot(mixed_all, mixout_all, preferred_element_type=jnp.float32) * mixout_scales
    residual_rows = (full_rows.astype(jnp.float32) + mix_term).astype(jnp.bfloat16)
    feature_count = tokens.shape[1]
    residual = lax.dynamic_slice_in_dim(
        residual_rows, lax.axis_index("tp") * feature_count, feature_count, 1
    )
    normed_ffn = rms_scaled(residual_rows, ffn_gain)
    gate_proj = add_rows(
        normed_ffn, lax.all_gather(w_gate.astype(jnp.bfloat16), "fs", axis=0, tiled=True)
    )
    up_proj = add_rows(
        normed_ffn, lax.all_gather(w_upward.astype(jnp.bfloat16), "fs", axis=0, tiled=True)
    )
    hidden = (jax.nn.silu(gate_proj * scale_gate) * (up_proj * scale_upward)).astype(jnp.bfloat16)
    down_terms = (
        jnp.dot(
            hidden,
            lax.all_gather(w_down.astype(jnp.bfloat16), "fs", axis=1, tiled=True),
            preferred_element_type=jnp.float32,
        )
        * down_scales
    )
    ffn_share = lax.psum_scatter(
        down_terms.astype(jnp.bfloat16), "tp", scatter_dimension=1, tiled=True
    ).astype(jnp.float32)
    return (residual.astype(jnp.float32) + ffn_share).astype(jnp.bfloat16)


def solution(mesh):
    in_specs = (
        P("fs", "tp"),
        P(),
        P(),
        P("fs", "tp"),
        P("fs", "tp"),
        P("fs", "tp"),
        P(None, "tp"),
        P(None, "tp"),
        P(None, "tp"),
        P(None, "tp"),
        P("tp", "fs"),
        P(None, "fs"),
        P("fs", "tp"),
        P("fs", "tp"),
        P(None, "tp"),
        P(None, "tp"),
        P("tp", "fs"),
        P(None, "fs"),
    )
    out_specs = P("fs", "tp")
    return jax.shard_map(
        per_device, mesh=mesh, in_specs=in_specs, out_specs=out_specs, check_vma=False
    )
```

profile of v0, /device:TPU:0, one launch (start us, length us, event | category | flops | bytes accessed | tf_op | source)
XLA Modules:
  0.0 623.6 jit_solution(6061713341310638662)
XLA Ops:
  6.5 0.0 copy-start.8
  6.5 0.0 copy-start.6
  6.5 0.0 all-gather.21.cloned.1.call-start
  6.5 1.6 convert_element_type.63
  8.2 0.0 all-gather.21.cloned.1.call-update
  8.2 0.0 all-gather.11.cloned.1.call-start
  8.2 0.7 all-gather.11.cloned.1.call-update
  8.9 0.0 all-gather.17.cloned.1.call-start
  9.0 1.6 convert_element_type.61
  10.6 0.0 all-gather.17.cloned.1.call-update
  10.6 0.0 all-gather.15.cloned.1.call-start
  10.7 1.6 convert_element_type.60
  12.3 0.0 all-gather.15.cloned.1.call-update
  12.3 0.0 all-gather.13.cloned.1.call-start
  12.4 1.6 convert_element_type.59
  14.0 0.0 all-gather.13.cloned.1.call-update
  14.0 0.0 all-gather.23.cloned.1.call-start
  14.0 37.5 %all-gather.21.cloned.1.call-done = bf16[256,2048]{1,0:T(8,128)(2,1)} async-done(((bf16[256,256]{1,0:T(8,128)(2,1)}), bf16[256,2048]{1,0:T(8,128)(2,1)}) %all-gather.21.cloned.1.call-update) | async-done | bytes 1048592 | tf_op jit(solution)/shard_map/all_gather | solution.py:73
  51.5 0.0 all-gather.23.cloned.1.call-update
  51.6 0.0 all-gather.19.cloned.1.call-start
  51.6 0.8 fusion.20
  52.4 34.2 %all-gather.11.cloned.1.call-done = bf16[1024,2048]{1,0:T(8,128)(2,1)} async-done(((bf16[1024,512]{1,0:T(8,128)(2,1)}), bf16[1024,2048]{1,0:T(8,128)(2,1)}) %all-gather.11.cloned.1.call-update) | async-done | bytes 4194320 | tf_op jit(solution)/shard_map/all_gather | solution.py:48
  86.6 3.1 fusion.3
  89.7 39.4 %all-gather.17.cloned.1.call-done = bf16[2048,256]{1,0:T(8,128)(2,1)} async-done(((bf16[256,256]{1,0:T(8,128)(2,1)}), bf16[2048,256]{1,0:T(8,128)(2,1)}) %all-gather.17.cloned.1.call-update) | async-done | bytes 1048592 | tf_op jit(solution)/shard_map/all_gather | solution.py:61
  129.0 0.0 copy-done.8
  129.0 0.0 copy-done.6
  129.0 3.8 convolution_multiply_fusion
  132.9 37.2 %all-gather.15.cloned.1.call-done = bf16[2048,256]{1,0:T(8,128)(2,1)} async-done(((bf16[256,256]{1,0:T(8,128)(2,1)}), bf16[2048,256]{1,0:T(8,128)(2,1)}) %all-gather.15.cloned.1.call-update) | async-done | bytes 1048592 | tf_op jit(solution)/shard_map/all_gather | solution.py:60
  170.0 0.0 copy-done.9
  170.0 3.8 fusion.8
  173.9 1.3 fusion.15
  175.2 35.9 %all-gather.13.cloned.1.call-done = bf16[2048,256]{1,0:T(8,128)(2,1)} async-done(((bf16[256,256]{1,0:T(8,128)(2,1)}), bf16[2048,256]{1,0:T(8,128)(2,1)}) %all-gather.13.cloned.1.call-update) | async-done | bytes 1048592 | tf_op jit(solution)/shard_map/all_gather | solution.py:59
  211.0 0.0 copy-done.10
  211.0 5.1 fusion.9
  216.1 0.0 all-gather.19.cloned.1.call-update
  216.2 0.0 all-gather.25.cloned.1.call-start
  216.2 0.0 copy-done
  216.2 1.0 convert_element_type.68
  217.2 0.0 all-gather.25.cloned.1.call-update
  217.2 0.0 all-gather.27.cloned.1.call-start
  217.3 0.0 copy-done.1
  217.3 1.0 convert_element_type.69
  218.2 0.0 all-gather.27.cloned.1.call-update
  218.3 0.0 all-gather.29.cloned.1.call-start
  218.3 2.5 convert_element_type.71
  220.8 0.0 all-gather.29.cloned.1.call-update
  220.8 0.0 reduce-scatter.2.cloned.1.call-start
  220.8 0.0 copy-done.2
  220.9 0.0 copy-done.3
  220.9 0.0 copy-done.4
  220.9 18.2 %all_gather.43 = f32[1,2048]{1,0:T(1,128)S(1)} all-gather(f32[1,256]{1,0:T(1,128)S(1)} %copy-done.4), channel_id=1, replica_groups=mesh['fs'=8,'tp'=4] {'fs'}, dimensions={1}, use_global_device_ids=true | all-gather | bytes 9216 | tf_op jit(solution)/shard_map/all_gather | solution.py:68
  239.1 0.0 copy-done.5
  239.1 16.6 %all_gather.47 = f32[1,2048]{1,0:T(1,128)S(1)} all-gather(f32[1,256]{1,0:T(1,128)S(1)} %copy-done.5), channel_id=1, replica_groups=mesh['fs'=8,'tp'=4] {'fs'}, dimensions={1}, use_global_device_ids=true | all-gather | bytes 9216 | tf_op jit(solution)/shard_map/all_gather | solution.py:69
  255.7 14.3 %all-gather.19.cloned.1.call-done = bf16[1024,1024]{1,0:T(8,128)(2,1)} async-done(((bf16[1024,256]{1,0:T(8,128)(2,1)}), bf16[1024,1024]{1,0:T(8,128)(2,1)}) %all-gather.19.cloned.1.call-update) | async-done | bytes 2097168 | tf_op jit(solution)/shard_map/all_gather | solution.py:72
  270.1 10.9 %fusion = (f32[1024]{0:T(1024)S(1)}, bf16[1024,2048]{1,0:T(8,128)(2,1)}) fusion(f32[2048]{0:T(1024)S(1)} %bitcast.26, bf16[1024,1024]{1,0:T(8,128)(2,1)} %all-gather.19.cloned.1.call-done, bf16[1024,2048]{1,0:T(8,128)(2,1)} %all-gather.23.cloned.1.call-done, bf16[1024,2048]{1,0:T(8,128)(2,1)} %all-gather.11.cloned.1.call-done), kind=kOutput, calls=%fused_computation.5 | convolution fusion | flops 4309646336 | bytes 14692352 | tf_op jit(solution)/shard_map/dot_general | solution.py:75
  281.0 83.6 %all-gather.25.cloned.1.call-done = bf16[2048,1408]{1,0:T(8,128)(2,1)} async-done(((bf16[256,1408]{1,0:T(8,128)(2,1)}), bf16[2048,1408]{1,0:T(8,128)(2,1)}) %all-gather.25.cloned.1.call-update) | async-done | bytes 5767184 | tf_op jit(solution)/shard_map/all_gather | solution.py:83
  364.6 0.0 copy-done.7
  364.6 11.9 %fusion.11 = f32[1024,1408]{1,0:T(8,128)} fusion(bf16[2048,1408]{1,0:T(8,128)(2,1)} %all-gather.25.cloned.1.call-done, bf16[1024,2048]{1,0:T(8,128)(2,1)} %get-tuple-element.9, f32[2048]{0:T(1024)S(1)} %copy-done.7, f32[1024]{0:T(1024)S(1)} %add_rsqrt_fusion), kind=kOutput, calls=%fused_computation.21 | convolution fusion | flops 5913968640 | bytes 15740928 | tf_op jit(solution)/shard_map/dot_general | solution.py:16
  376.5 80.8 %all-gather.27.cloned.1.call-done = bf16[2048,1408]{1,0:T(8,128)(2,1)} async-done(((bf16[256,1408]{1,0:T(8,128)(2,1)}), bf16[2048,1408]{1,0:T(8,128)(2,1)}) %all-gather.27.cloned.1.call-update) | async-done | bytes 5767184 | tf_op jit(solution)/shard_map/all_gather | solution.py:86
  457.3 93.2 %all-gather.29.cloned.1.call-done = bf16[1408,2048]{1,0:T(8,128)(2,1)} async-done(((bf16[1408,256]{1,0:T(8,128)(2,1)}), bf16[1408,2048]{1,0:T(8,128)(2,1)}) %all-gather.29.cloned.1.call-update) | async-done | bytes 5767184 | tf_op jit(solution)/shard_map/all_gather | solution.py:92
  550.5 21.0 %multiply_convert_fusion = bf16[1024,2048]{1,0:T(8,128)(2,1)} fusion(bf16[1408,2048]{1,0:T(8,128)(2,1)} %all-gather.29.cloned.1.call-done, f32[2048]{0:T(1024)S(1)} %bitcast.25, f32[1024,1408]{1,0:T(8,128)} %fusion.11, bf16[2048,1408]{1,0:T(8,128)(2,1)} %all-gather.27.cloned.1.call-done, f32[1408]{0:T(1024)S(1)} %reduce.1, f32[1408]{0:T(1024)S(1)} %reduce, ...), kind=kOutput, calls=%fused_computation.12 | convolution fusion | flops 11835277312 | bytes 25721856 | tf_op jit(solution)/shard_map/dot_general | solution.py:90
  571.5 0.0 reduce-scatter.2.cloned.1.call-update
  571.6 42.7 %reduce-scatter.2.cloned.1.call-done = bf16[1024,512]{1,0:T(8,128)(2,1)} async-done(((bf16[1024,2048]{1,0:T(8,128)(2,1)}), bf16[1024,512]{1,0:T(8,128)(2,1)}) %reduce-scatter.2.cloned.1.call-update) | async-done | bytes 1048592 | tf_op jit(solution)/shard_map/reduce_scatter | solution.py:97
  614.3 2.8 add_convert_fusion
  (14 shorter events, 0.1 us)
Async XLA Ops:
  6.5 122.5 %copy-start.8 = (f32[1,256]{1,0:T(1,128)S(1)}, f32[1,256]{1,0:T(1,128)}, u32[]{:S(2)}) copy-start(f32[1,256]{1,0:T(1,128)} %param.26) | copy-start | bytes 3076
  6.5 122.5 %copy-start.6 = (f32[2048]{0:T(1024)S(1)}, f32[2048]{0:T(1024)}, u32[]{:S(2)}) copy-start(f32[2048]{0:T(1024)} %param.19) | copy-start | bytes 24580
  6.5 45.0 %all-gather.21.cloned.1.call-start = ((), (), s32[]{:S(2)}) async-start(), calls=%async_computation.6 | async-start | bytes 1179648 | tf_op jit(solution)/shard_map/all_gather | solution.py:73
  8.2 78.4 %all-gather.11.cloned.1.call-start = ((), (), s32[]{:S(2)}) async-start(), calls=%async_computation.1 | async-start | bytes 5242880 | tf_op jit(solution)/shard_map/all_gather | solution.py:48
  8.9 120.1 %all-gather.17.cloned.1.call-start = ((), (), s32[]{:S(2)}) async-start(), calls=%async_computation.4 | async-start | bytes 1179648 | tf_op jit(solution)/shard_map/all_gather | solution.py:61
  10.6 159.4 %all-gather.15.cloned.1.call-start = ((), (), s32[]{:S(2)}) async-start(), calls=%async_computation.3 | async-start | bytes 1179648 | tf_op jit(solution)/shard_map/all_gather | solution.py:60
  12.3 198.7 %all-gather.13.cloned.1.call-start = ((), (), s32[]{:S(2)}) async-start(), calls=%async_computation.2 | async-start | bytes 1179648 | tf_op jit(solution)/shard_map/all_gather | solution.py:59
  14.0 241.7 %all-gather.23.cloned.1.call-start = ((), (), s32[]{:S(2)}) async-start(), calls=%async_computation.7 | async-start | bytes 5242880 | tf_op jit(solution)/shard_map/all_gather | solution.py:74
  51.6 218.5 %all-gather.19.cloned.1.call-start = ((), (), s32[]{:S(2)}) async-start(), calls=%async_computation.5 | async-start | bytes 2621440 | tf_op jit(solution)/shard_map/all_gather | solution.py:72
  129.0 41.0 %copy-start.9 = (f32[1,256]{1,0:T(1,128)S(1)}, f32[1,256]{1,0:T(1,128)}, u32[]{:S(2)}) copy-start(f32[1,256]{1,0:T(1,128)} %param.25) | copy-start | bytes 3076
  170.0 41.0 %copy-start.10 = (f32[1,256]{1,0:T(1,128)S(1)}, f32[1,256]{1,0:T(1,128)}, u32[]{:S(2)}) copy-start(f32[1,256]{1,0:T(1,128)} %param.24) | copy-start | bytes 3076
  211.0 5.2 copy-start
  211.0 6.2 copy-start.1
  216.1 4.7 copy-start.2
  216.1 4.8 copy-start.3
  216.1 4.8 copy-start.4
  216.1 23.0 %copy-start.5 = (f32[1,256]{1,0:T(1,128)S(1)}, f32[1,256]{1,0:T(1,128)}, u32[]{:S(2)}) copy-start(f32[1,256]{1,0:T(1,128)} %param.35) | copy-start | bytes 3076
  216.2 148.4 %all-gather.25.cloned.1.call-start = ((), (), s32[]{:S(2)}) async-start(), calls=%async_computation.8 | async-start | bytes 6488064 | tf_op jit(solution)/shard_map/all_gather | solution.py:83
  217.2 240.1 %all-gather.27.cloned.1.call-start = ((), (), s32[]{:S(2)}) async-start(), calls=%async_computation.9 | async-start | bytes 6488064 | tf_op jit(solution)/shard_map/all_gather | solution.py:86
  218.3 332.3 %all-gather.29.cloned.1.call-start = ((), (), s32[]{:S(2)}) async-start(), calls=%async_computation.10 | async-start | bytes 6488064 | tf_op jit(solution)/shard_map/all_gather | solution.py:92
  220.8 393.5 %reduce-scatter.2.cloned.1.call-start = ((), (), s32[]{:S(2)}) async-start(), calls=%async_computation.11 | async-start | bytes 5242880 | tf_op jit(solution)/shard_map/reduce_scatter | solution.py:97
  270.0 94.5 %copy-start.7 = (f32[2048]{0:T(1024)S(1)}, f32[2048]{0:T(1024)}, u32[]{:S(2)}) copy-start(f32[2048]{0:T(1024)} %param.20) | copy-start | bytes 24580
Sparse Core Ops, SparseCore 0:
  9.4 42.1 all-gather.20
  53.1 33.4 all-gather.10
  88.7 40.2 all-gather.16
  131.0 38.9 all-gather.14
  172.0 38.9 all-gather.12
  212.5 33.1 all-gather.22
  247.2 22.8 all-gather.18
  272.2 92.2 all-gather.24
  366.8 90.4 all-gather.26
  459.2 91.2 all-gather.28
  571.7 42.5 reduce-scatter.1
where the time goes:
time: 624 us
  waiting for transfers between devices  500 us (80%)
  matrix products  56.6 us (9%)
  blocking collectives  34.8 us (6%)
  other arithmetic  18 us (3%)
  between operations  13.3 us (2%)
    all_gather x1, waiting for transfers between devices, per_device(): lax.all_gather(w_down.astype(jnp.bfloat16), 'fs', axis=1, tiled=True)  93.2 us
    all_gather x1, waiting for transfers between devices, per_device(): lax.all_gather(w_gate.astype(jnp.bfloat16), 'fs', axis=0, tiled=True)  83.6 us
    all_gather x1, waiting for transfers between devices, per_device(): lax.all_gather(w_upward.astype(jnp.bfloat16), 'fs', axis=0, tiled=True)  80.8 us
    reduce_scatter x1, waiting for transfers between devices, per_device(): lax.psum_scatter(down_terms.astype(jnp.bfloat16), 'tp', scatter_dimension...  42.7 us
    all_gather x1, waiting for transfers between devices, per_device(): value = add_one(lax.all_gather(value_bf, 'fs', axis=0, tiled=True))  39.4 us
    all_gather x1, waiting for transfers between devices, per_device(): mixout_cols = lax.all_gather(mixout_bf, 'fs', axis=1, tiled=True)  37.5 us
    all_gather x1, waiting for transfers between devices, per_device(): inner = add_one(lax.all_gather(inner_bf, 'fs', axis=0, tiled=True))  37.2 us
    all_gather x1, waiting for transfers between devices, per_device(): outer = add_one(lax.all_gather(outer_bf, 'fs', axis=0, tiled=True))  35.9 us
  transfers between devices with their start and end apart: 11, of which 10 were waited for; matrix products, arithmetic and copies ran while one was open for 8% of the time, Pallas kernels for 0%

commit v1 on v0

--- a/solution.py
+++ b/solution.py
@@ -45,7 +45,12 @@
     w_down,
     scale_down,
 ):
-    full_rows = lax.all_gather(tokens, "tp", axis=1, tiled=True)
+    ring = [tokens]
+    for hop in range(3):
+        ring.append(lax.ppermute(ring[-1], "tp", [(dev, (dev + 1) % 4) for dev in range(4)]))
+    full_rows = jnp.roll(
+        jnp.concatenate(ring[::-1], axis=1), (lax.axis_index("tp") + 1) * ring[0].shape[1], axis=1
+    )
     normed = rms_scaled(full_rows, mixer_gain)
     tok_count = tokens.shape[0]
     local_channels = w_outer.shape[1]

time: 624 us -> 588 us (0.942)
  waiting for transfers between devices: 500 us -> 458 us
  local copies, waits for them, and re-layouts: 0.85 us -> 7.8 us
    all_gather x1, waiting for transfers between devices: 39.4 us -> 0.02 us  [per_device(): value = add_one(lax.all_gather(value_bf, 'fs', axis=0, tiled=True))]
    ppermute x0 -> x3, waiting for transfers between devices: none -> 38.9 us  [per_device(): lax.ppermute(ring[-1], 'tp', [(dev, (dev + 1) % 4) for dev in range(4)])]
    all_gather x1 -> x0, waiting for transfers between devices: 34.2 us -> none  [per_device(): full_rows = lax.all_gather(tokens, 'tp', axis=1, tiled=True)]
    all_gather x1, waiting for transfers between devices: 0.01 us -> 19.7 us  [per_device(): mixout_all = lax.all_gather(mixout_cols, 'tp', axis=0, tiled=True)]
    all_gather x1, waiting for transfers between devices: 14.3 us -> 0.01 us  [per_device(): mixed_all = lax.all_gather(mixed_out, 'tp', axis=1, tiled=True)]
    all_gather x1, waiting for transfers between devices: 37.2 us -> 28.1 us  [per_device(): inner = add_one(lax.all_gather(inner_bf, 'fs', axis=0, tiled=True))]
    unnamed x22 -> x33, local copies, waits for them, and re-layouts: 0.04 us -> 6.84 us
  transfers between devices with their start and end apart: 11 -> 13, of which waited for: 10 -> 11; matrix products, arithmetic and copies ran while one was open for 8% -> 9% of each run, Pallas kernels for 0% -> 0%
where the time goes in v1:
time: 588 us
  waiting for transfers between devices  458 us (78%)
  matrix products  56.6 us (10%)
  blocking collectives  34.9 us (6%)
  other arithmetic  15.8 us (3%)
  between operations  13.8 us (2%)
  local copies, waits for them, and re-layouts  7.8 us (1%)
    all_gather x1, waiting for transfers between devices, per_device(): lax.all_gather(w_down.astype(jnp.bfloat16), 'fs', axis=1, tiled=True)  93.4 us
    all_gather x1, waiting for transfers between devices, per_device(): lax.all_gather(w_gate.astype(jnp.bfloat16), 'fs', axis=0, tiled=True)  83.6 us
    all_gather x1, waiting for transfers between devices, per_device(): lax.all_gather(w_upward.astype(jnp.bfloat16), 'fs', axis=0, tiled=True)  80.8 us
    reduce_scatter x1, waiting for transfers between devices, per_device(): lax.psum_scatter(down_terms.astype(jnp.bfloat16), 'tp', scatter_dimension...  42.7 us
    ppermute x3, waiting for transfers between devices, per_device(): lax.ppermute(ring[-1], 'tp', [(dev, (dev + 1) % 4) for dev in range(4)])  38.9 us
    all_gather x1, waiting for transfers between devices, per_device(): outer = add_one(lax.all_gather(outer_bf, 'fs', axis=0, tiled=True))  36 us
    all_gather x1, waiting for transfers between devices, per_device(): mixout_cols = lax.all_gather(mixout_bf, 'fs', axis=1, tiled=True)  34.9 us
    all_gather x1, waiting for transfers between devices, per_device(): inner = add_one(lax.all_gather(inner_bf, 'fs', axis=0, tiled=True))  28.1 us
  transfers between devices with their start and end apart: 13, of which 11 were waited for; matrix products, arithmetic and copies ran while one was open for 9% of the time, Pallas kernels for 0%

profile of v1, /device:TPU:0, one launch (start us, length us, event | category | flops | bytes accessed | tf_op | source)
XLA Modules:
  0.0 588.0 jit_solution(17406532916929388863)
XLA Ops:
  6.5 1.7 convert_element_type.61
  8.2 0.0 all-gather.14.cloned.1.call-update
  8.3 0.0 all-gather.12.cloned.1.call-start
  8.3 1.6 convert_element_type.60
  9.9 0.0 all-gather.12.cloned.1.call-update
  10.0 0.0 all-gather.10.cloned.1.call-start
  10.0 0.5 collective-permute-start
  10.6 14.6 %collective-permute-done = bf16[1024,512]{1,0:T(8,128)(2,1)S(1)} collective-permute-done((bf16[1024,512]{1,0:T(8,128)(2,1)}, bf16[1024,512]{1,0:T(8,128)(2,1)S(1)}, u32[]{:S(2)}, u32[]{:S(2)}) %collective-permute-start) | collective-permute-done | bytes 1048608 | tf_op jit(solution)/shard_map/ppermute | solution.py:50
  25.2 0.0 collective-permute-start.1
  25.2 1.6 convert_element_type.59
  26.8 0.0 all-gather.10.cloned.1.call-update
  26.9 0.0 all-gather.18.cloned.1.call-start
  26.9 12.5 %collective-permute-done.1 = bf16[1024,512]{1,0:T(8,128)(2,1)S(1)} collective-permute-done((bf16[1024,512]{1,0:T(8,128)(2,1)S(1)}, bf16[1024,512]{1,0:T(8,128)(2,1)S(1)}, u32[]{:S(2)}, u32[]{:S(2)}) %collective-permute-start.1) | collective-permute-done | bytes 1048608 | tf_op jit(solution)/shard_map/ppermute | solution.py:50
  39.4 1.6 convert_element_type.63
  41.0 0.0 all-gather.18.cloned.1.call-update
  41.1 0.0 all-gather.16.cloned.1.call-start
  41.1 0.8 fusion.20
  41.9 11.8 %collective-permute-done.2 = bf16[1024,512]{1,0:T(8,128)(2,1)} collective-permute-done((bf16[1024,512]{1,0:T(8,128)(2,1)S(1)}, bf16[1024,512]{1,0:T(8,128)(2,1)}, u32[]{:S(2)}, u32[]{:S(2)}) %collective-permute-start.2) | collective-permute-done | bytes 1048608 | tf_op jit(solution)/shard_map/ppermute | solution.py:50
  53.7 1.4 constant_dynamic-update-slice_fusion.7
  55.1 0.2 constant_dynamic-update-slice_fusion.6
  55.3 0.2 constant_dynamic-update-slice_fusion.5
  55.4 0.1 constant_dynamic-update-slice_fusion.4
  55.6 1.4 constant_dynamic-update-slice_fusion.3
  57.0 0.0 copy-start.8
  57.0 0.0 copy-start.10
  57.0 0.1 constant_dynamic-update-slice_fusion.2
  57.2 0.2 constant_dynamic-update-slice_fusion.1
  57.3 0.2 constant_dynamic-update-slice_fusion
  57.5 3.3 copy-done.1
  60.8 0.9 fusion.3
  61.7 0.0 all-gather.14.cloned.1.call-done
  61.7 0.0 copy-start.11
  61.7 3.8 convolution_multiply_fusion
  65.5 28.1 %all-gather.12.cloned.1.call-done = bf16[2048,256]{1,0:T(8,128)(2,1)} async-done(((bf16[256,256]{1,0:T(8,128)(2,1)}), bf16[2048,256]{1,0:T(8,128)(2,1)}) %all-gather.12.cloned.1.call-update) | async-done | bytes 1048592 | tf_op jit(solution)/shard_map/all_gather | solution.py:65
  93.6 3.8 fusion.8
  97.5 1.3 fusion.15
  98.8 36.0 %all-gather.10.cloned.1.call-done = bf16[2048,256]{1,0:T(8,128)(2,1)} async-done(((bf16[256,256]{1,0:T(8,128)(2,1)}), bf16[2048,256]{1,0:T(8,128)(2,1)}) %all-gather.10.cloned.1.call-update) | async-done | bytes 1048592 | tf_op jit(solution)/shard_map/all_gather | solution.py:64
  134.8 5.1 fusion.9
  139.9 0.0 all-gather.16.cloned.1.call-update
  139.9 0.0 all-gather.20.cloned.1.call-start
  140.0 34.9 %all-gather.18.cloned.1.call-done = bf16[256,2048]{1,0:T(8,128)(2,1)} async-done(((bf16[256,256]{1,0:T(8,128)(2,1)}), bf16[256,2048]{1,0:T(8,128)(2,1)}) %all-gather.18.cloned.1.call-update) | async-done | bytes 1048592 | tf_op jit(solution)/shard_map/all_gather | solution.py:78
  174.8 0.0 all-gather.20.cloned.1.call-update
  174.9 0.0 all-gather.22.cloned.1.call-start
  174.9 0.9 convert_element_type.68
  175.9 0.0 all-gather.22.cloned.1.call-update
  175.9 0.0 all-gather.24.cloned.1.call-start
  175.9 1.0 convert_element_type.69
  176.9 0.0 all-gather.24.cloned.1.call-update
  176.9 0.0 all-gather.26.cloned.1.call-start
  177.0 2.3 convert_element_type.71
  179.3 0.0 all-gather.26.cloned.1.call-update
  179.3 0.0 reduce-scatter.2.cloned.1.call-start
  179.4 18.4 %all_gather.39 = f32[1,2048]{1,0:T(1,128)S(1)} all-gather(f32[1,256]{1,0:T(1,128)S(1)} %copy-done.6), channel_id=1, replica_groups=mesh['fs'=8,'tp'=4] {'fs'}, dimensions={1}, use_global_device_ids=true | all-gather | bytes 9216 | tf_op jit(solution)/shard_map/all_gather | solution.py:73
  197.8 16.5 %all_gather.43 = f32[1,2048]{1,0:T(1,128)S(1)} all-gather(f32[1,256]{1,0:T(1,128)S(1)} %copy-done.7), channel_id=1, replica_groups=mesh['fs'=8,'tp'=4] {'fs'}, dimensions={1}, use_global_device_ids=true | all-gather | bytes 9216 | tf_op jit(solution)/shard_map/all_gather | solution.py:74
  214.3 19.7 %all-gather.20.cloned.1.call-done = bf16[1024,2048]{1,0:T(8,128)(2,1)} async-done(((bf16[256,2048]{1,0:T(8,128)(2,1)}), bf16[1024,2048]{1,0:T(8,128)(2,1)}) %all-gather.20.cloned.1.call-update) | async-done | bytes 4194320 | tf_op jit(solution)/shard_map/all_gather | solution.py:79
  234.0 10.9 %fusion = (f32[1024]{0:T(1024)S(1)}, bf16[1024,2048]{1,0:T(8,128)(2,1)}) fusion(f32[2048]{0:T(1024)S(1)} %bitcast.26, bf16[1024,1024]{1,0:T(8,128)(2,1)} %all-gather.16.cloned.1.call-done, bf16[1024,2048]{1,0:T(8,128)(2,1)} %all-gather.20.cloned.1.call-done, bf16[1024,4096]{1,0:T(8,128)(2,1)} %copy-done.1, s32[]{:T(128)S(6)} %select_n.17), kind=kOutput, calls=%fused_computation.5 | convolution fusion | flops 4309646336 | bytes 14692356 | tf_op jit(solution)/shard_map/dot_general | solution.py:80
  244.9 83.6 %all-gather.22.cloned.1.call-done = bf16[2048,1408]{1,0:T(8,128)(2,1)} async-done(((bf16[256,1408]{1,0:T(8,128)(2,1)}), bf16[2048,1408]{1,0:T(8,128)(2,1)}) %all-gather.22.cloned.1.call-update) | async-done | bytes 5767184 | tf_op jit(solution)/shard_map/all_gather | solution.py:88
  328.5 11.9 %fusion.11 = f32[1024,1408]{1,0:T(8,128)} fusion(bf16[2048,1408]{1,0:T(8,128)(2,1)} %all-gather.22.cloned.1.call-done, bf16[1024,2048]{1,0:T(8,128)(2,1)} %get-tuple-element.9, f32[2048]{0:T(1024)S(1)} %copy-done.9, f32[1024]{0:T(1024)S(1)} %add_rsqrt_fusion), kind=kOutput, calls=%fused_computation.21 | convolution fusion | flops 5913968640 | bytes 15740928 | tf_op jit(solution)/shard_map/dot_general | solution.py:16
  340.5 80.8 %all-gather.24.cloned.1.call-done = bf16[2048,1408]{1,0:T(8,128)(2,1)} async-done(((bf16[256,1408]{1,0:T(8,128)(2,1)}), bf16[2048,1408]{1,0:T(8,128)(2,1)}) %all-gather.24.cloned.1.call-update) | async-done | bytes 5767184 | tf_op jit(solution)/shard_map/all_gather | solution.py:91
  421.2 93.4 %all-gather.26.cloned.1.call-done = bf16[1408,2048]{1,0:T(8,128)(2,1)} async-done(((bf16[1408,256]{1,0:T(8,128)(2,1)}), bf16[1408,2048]{1,0:T(8,128)(2,1)}) %all-gather.26.cloned.1.call-update) | async-done | bytes 5767184 | tf_op jit(solution)/shard_map/all_gather | solution.py:97
  514.6 21.0 %multiply_convert_fusion = bf16[1024,2048]{1,0:T(8,128)(2,1)} fusion(bf16[1408,2048]{1,0:T(8,128)(2,1)} %all-gather.26.cloned.1.call-done, f32[2048]{0:T(1024)S(1)} %bitcast.25, f32[1024,1408]{1,0:T(8,128)} %fusion.11, bf16[2048,1408]{1,0:T(8,128)(2,1)} %all-gather.24.cloned.1.call-done, f32[1408]{0:T(1024)S(1)} %reduce.1, f32[1408]{0:T(1024)S(1)} %reduce, ...), kind=kOutput, calls=%fused_computation.12 | convolution fusion | flops 11835277312 | bytes 25721856 | tf_op jit(solution)/shard_map/dot_general | solution.py:95
  535.6 0.0 reduce-scatter.2.cloned.1.call-update
  535.7 42.7 %reduce-scatter.2.cloned.1.call-done = bf16[1024,512]{1,0:T(8,128)(2,1)} async-done(((bf16[1024,2048]{1,0:T(8,128)(2,1)}), bf16[1024,512]{1,0:T(8,128)(2,1)}) %reduce-scatter.2.cloned.1.call-update) | async-done | bytes 1048592 | tf_op jit(solution)/shard_map/reduce_scatter | solution.py:102
  578.4 2.8 add_convert_fusion
  (29 shorter events, 0.1 us)
Async XLA Ops:
  6.5 48.9 %copy-start = (bf16[1024,512]{1,0:T(8,128)(2,1)S(1)}, bf16[1024,512]{1,0:T(8,128)(2,1)}, u32[]{:S(2)}) copy-start(bf16[1024,512]{1,0:T(8,128)(2,1)} %param.18) | copy-start | bytes 3145732
  6.5 55.2 %all-gather.14.cloned.1.call-start = ((), (), s32[]{:S(2)}) async-start(), calls=%async_computation.3 | async-start | bytes 1179648 | tf_op jit(solution)/shard_map/all_gather | solution.py:66
  8.3 85.4 %all-gather.12.cloned.1.call-start = ((), (), s32[]{:S(2)}) async-start(), calls=%async_computation.2 | async-start | bytes 1179648 | tf_op jit(solution)/shard_map/all_gather | solution.py:65
  10.0 124.8 %all-gather.10.cloned.1.call-start = ((), (), s32[]{:S(2)}) async-start(), calls=%async_computation.1 | async-start | bytes 1179648 | tf_op jit(solution)/shard_map/all_gather | solution.py:64
  10.0 15.2 %collective-permute-start = (bf16[1024,512]{1,0:T(8,128)(2,1)}, bf16[1024,512]{1,0:T(8,128)(2,1)S(1)}, u32[]{:S(2)}, u32[]{:S(2)}) collective-permute-start(bf16[1024,512]{1,0:T(8,128)(2,1)} %param.18), channel_id=1, source_target_pairs={{0,1},{1,2},{2,3},{3,0},{4,5},{5,6},{6,7},{7,4},{8,9},{9,10},{10,1... | collective-permute-start | bytes 3145736 | tf_op jit(solution)/shard_map/ppermute | solution.py:50
  25.2 14.2 %collective-permute-start.1 = (bf16[1024,512]{1,0:T(8,128)(2,1)S(1)}, bf16[1024,512]{1,0:T(8,128)(2,1)S(1)}, u32[]{:S(2)}, u32[]{:S(2)}) collective-permute-start(bf16[1024,512]{1,0:T(8,128)(2,1)S(1)} %collective-permute-done), channel_id=1, source_target_pairs={{0,1},{1,2},{2,3},{3,0},{4,5},{5,6},{6,7},{7,4},{8,9},{9,10},{10,1... | collective-permute-start | bytes 3145736 | tf_op jit(solution)/shard_map/ppermute | solution.py:50
  26.9 148.0 %all-gather.18.cloned.1.call-start = ((), (), s32[]{:S(2)}) async-start(), calls=%async_computation.5 | async-start | bytes 1179648 | tf_op jit(solution)/shard_map/all_gather | solution.py:78
  39.4 14.3 %collective-permute-start.2 = (bf16[1024,512]{1,0:T(8,128)(2,1)S(1)}, bf16[1024,512]{1,0:T(8,128)(2,1)}, u32[]{:S(2)}, u32[]{:S(2)}) collective-permute-start(bf16[1024,512]{1,0:T(8,128)(2,1)S(1)} %collective-permute-done.1), channel_id=1, source_target_pairs={{0,1},{1,2},{2,3},{3,0},{4,5},{5,6},{6,7},{7,4},{8,9},{9,10},{10,1... | collective-permute-start | bytes 3145736 | tf_op jit(solution)/shard_map/ppermute | solution.py:50
  41.1 173.2 %all-gather.16.cloned.1.call-start = ((), (), s32[]{:S(2)}) async-start(), calls=%async_computation.4 | async-start | bytes 2621440 | tf_op jit(solution)/shard_map/all_gather | solution.py:77
  57.0 4.7 copy-start.8
  57.0 4.7 copy-start.10
  57.5 3.3 copy-start.1
  61.7 31.9 %copy-start.11 = (f32[1,256]{1,0:T(1,128)S(1)}, f32[1,256]{1,0:T(1,128)}, u32[]{:S(2)}) copy-start(f32[1,256]{1,0:T(1,128)} %param.25) | copy-start | bytes 3076
  93.6 41.2 %copy-start.12 = (f32[1,256]{1,0:T(1,128)S(1)}, f32[1,256]{1,0:T(1,128)}, u32[]{:S(2)}) copy-start(f32[1,256]{1,0:T(1,128)} %param.24) | copy-start | bytes 3076
  134.8 40.1 %copy-start.2 = (f32[256,1408]{1,0:T(8,128)S(1)}, f32[256,1408]{1,0:T(8,128)}, u32[]{:S(2)}) copy-start(f32[256,1408]{1,0:T(8,128)} %param.30) | copy-start | bytes 4325380
  134.8 41.1 %copy-start.3 = (f32[256,1408]{1,0:T(8,128)S(1)}, f32[256,1408]{1,0:T(8,128)}, u32[]{:S(2)}) copy-start(f32[256,1408]{1,0:T(8,128)} %param.31) | copy-start | bytes 4325380
  139.9 39.5 %copy-start.4 = (f32[1,1408]{1,0:T(1,128)S(1)}, f32[1,1408]{1,0:T(1,128)}, u32[]{:S(2)}) copy-start(f32[1,1408]{1,0:T(1,128)} %param.32) | copy-start | bytes 16900
  139.9 39.5 %copy-start.5 = (f32[1,1408]{1,0:T(1,128)S(1)}, f32[1,1408]{1,0:T(1,128)}, u32[]{:S(2)}) copy-start(f32[1,1408]{1,0:T(1,128)} %param.33) | copy-start | bytes 16900
  139.9 39.5 %copy-start.6 = (f32[1,256]{1,0:T(1,128)S(1)}, f32[1,256]{1,0:T(1,128)}, u32[]{:S(2)}) copy-start(f32[1,256]{1,0:T(1,128)} %param.29) | copy-start | bytes 3076
  139.9 58.0 %copy-start.7 = (f32[1,256]{1,0:T(1,128)S(1)}, f32[1,256]{1,0:T(1,128)}, u32[]{:S(2)}) copy-start(f32[1,256]{1,0:T(1,128)} %param.35) | copy-start | bytes 3076
  139.9 94.1 %all-gather.20.cloned.1.call-start = ((), (), s32[]{:S(2)}) async-start(), calls=%async_computation.6 | async-start | bytes 5242880 | tf_op jit(solution)/shard_map/all_gather | solution.py:79
  174.9 153.7 %all-gather.22.cloned.1.call-start = ((), (), s32[]{:S(2)}) async-start(), calls=%async_computation.7 | async-start | bytes 6488064 | tf_op jit(solution)/shard_map/all_gather | solution.py:88
  175.9 245.3 %all-gather.24.cloned.1.call-start = ((), (), s32[]{:S(2)}) async-start(), calls=%async_computation.8 | async-start | bytes 6488064 | tf_op jit(solution)/shard_map/all_gather | solution.py:91
  176.9 337.7 %all-gather.26.cloned.1.call-start = ((), (), s32[]{:S(2)}) async-start(), calls=%async_computation.9 | async-start | bytes 6488064 | tf_op jit(solution)/shard_map/all_gather | solution.py:97
  179.3 399.1 %reduce-scatter.2.cloned.1.call-start = ((), (), s32[]{:S(2)}) async-start(), calls=%async_computation.10 | async-start | bytes 5242880 | tf_op jit(solution)/shard_map/reduce_scatter | solution.py:102
  234.0 94.5 %copy-start.9 = (f32[2048]{0:T(1024)S(1)}, f32[2048]{0:T(1024)}, u32[]{:S(2)}) copy-start(f32[2048]{0:T(1024)} %param.20) | copy-start | bytes 24580
Sparse Core Ops, SparseCore 0:
  9.5 42.9 all-gather.13
  54.6 38.9 all-gather.11
  95.8 38.9 all-gather.9
  136.7 38.0 all-gather.17
  176.2 21.8 all-gather.15
  199.5 34.4 all-gather.19
  236.2 92.2 all-gather.21
  330.7 90.4 all-gather.23
  423.3 91.2 all-gather.25
  535.8 42.5 reduce-scatter.1
